TPU v7x, 32 devices: a whole 2x2x4 slice. The times are simulated.
32 devices in a mesh: sp: 8 (over z, y), dp: 4 (over x, core).
Axes of the slice: x: 2, y: 2, z: 4, core: 2. Of those that a mesh axis runs over, the one named last changes fastest.
Arguments:
- stream: bfloat16 [4, 1024, 2048], P('dp', 'sp'), may hold values from -1.796875 to 1.796875
- query_rows: bfloat16 [4, 1024, 2048], P('dp', 'sp'), may hold values from -5 to 5
- key_rows: bfloat16 [4, 1024, 2048], P('dp', 'sp'), may hold values from -5 to 5
- value_rows: bfloat16 [4, 1024, 2048], P('dp', 'sp'), may hold values from -6 to 6
- forget_sums: float32 [4, 16, 1024], P('dp', 'sp'), may hold values from -1024 to 0, as said below
- out_weight: bfloat16 [2048, 2048], replicated, may hold values from -1.5 to 1.5
- first_gain: float32 [2048], replicated, may hold values from 0.1 to 1.9
- expert_ids: int32 [4, 1024, 4], P('dp', 'sp'), may hold values from 0 to 31, all different within a row; in each aligned block of 128 rows (0 to 127, 128 to 255, ..., all dimensions but the last counted through in order) at most 24 rows name the same one
- route_scores: float32 [4, 1024, 4], P('dp', 'sp'), may hold values from -6 to 6
- gate_weight: bfloat16 [32, 2048, 512], P(('sp', 'dp')), may hold values from -0.5 to 0.5
- up_weight: bfloat16 [32, 2048, 512], P(('sp', 'dp')), may hold values from -0.5 to 0.5
- down_weight: bfloat16 [32, 512, 2048], P(('sp', 'dp')), may hold values from -0.0625 to 0.0625
- second_gain: float32 [2048], replicated, may hold values from 0.1 to 1.9
Outputs:
- mixed_stream: bfloat16 [4, 1024, 2048], P('dp', 'sp')
Inputs may be any that keep to these rules, and one draw needn't show every extreme that they name: `expert_ids`: each row names 4 different experts; in the rows of one device no expert is named more than 24 times. `forget_sums`: along positions each head's values never rise.
All inputs are finite; a program needn't handle non-finite values.
Results may differ from a plain program's by a relative error of at most 0.0085.
Values may be sent and summed in bfloat16 or wider, within the bound.
A program may use at most 128 MiB of HBM per device.

v0:
```python
import jax
import jax.numpy as jnp
from jax import lax
from jax.sharding import PartitionSpec as P

deep_alpha = 8.0**0.25
clamp_limit = 7.0
swish_alpha = 1.702
norm_eps = 1e-05
mask_fill = -1e30


def layer_norm(summed, gain_row):
    centre = jnp.mean(summed, axis=-1, keepdims=True)
    spread = jnp.mean(jnp.square(summed - centre), axis=-1, keepdims=True)
    return (summed - centre) * lax.rsqrt(spread + norm_eps) * gain_row


def attend_local(query_all, key_all, value_all, gate_all):
    length, width = query_all.shape
    heads = gate_all.shape[0]
    head_size = width // heads
    query_split = query_all.reshape(length, heads, head_size)
    key_split = key_all.reshape(length, heads, head_size)
    value_split = value_all.reshape(length, heads, head_size)
    q_block = min(512, length)
    block_count = length // q_block
    inv_root = head_size ** (-0.5)
    key_pos = jnp.arange(length, dtype=jnp.int32)

    def one_block(block_index):
        first_row = block_index * q_block
        row_block = lax.dynamic_slice_in_dim(query_split, first_row, q_block, 0)
        row_gate = lax.dynamic_slice_in_dim(gate_all, first_row, q_block, 1)
        scores = (
            jnp.einsum("qhd,khd->hqk", row_block, key_split, preferred_element_type=jnp.float32)
            * inv_root
        )
        scores = scores + row_gate[:, :, None] - gate_all[:, None, :]
        query_pos = first_row + jnp.arange(q_block, dtype=jnp.int32)
        scores = jnp.where((query_pos[:, None] >= key_pos[None, :])[None], scores, mask_fill)
        row_max = jnp.max(scores, axis=2, keepdims=True)
        weights = jnp.exp(scores - row_max)
        row_total = jnp.sum(weights, axis=2)
        blended = jnp.einsum(
            "hqk,khd->qhd",
            weights.astype(jnp.bfloat16),
            value_split,
            preferred_element_type=jnp.float32,
        )
        return (blended / row_total.T[:, :, None]).astype(jnp.bfloat16)

    return lax.map(one_block, jnp.arange(block_count, dtype=jnp.int32)).reshape(length, width)


def expert_rows(row_block, gate_matrix, up_matrix, down_matrix):
    gate_act = jnp.minimum(
        jnp.dot(row_block, gate_matrix, preferred_element_type=jnp.float32), clamp_limit
    )
    up_act = jnp.clip(
        jnp.dot(row_block, up_matrix, preferred_element_type=jnp.float32), -clamp_limit, clamp_limit
    )
    hidden = (gate_act * jax.nn.sigmoid(swish_alpha * gate_act) * (up_act + 1.0)).astype(
        jnp.bfloat16
    )
    return jnp.dot(hidden, down_matrix, preferred_element_type=jnp.float32).astype(jnp.bfloat16)


def shards(
    stream,
    query_rows,
    key_rows,
    value_rows,
    forget_sums,
    out_weight,
    first_gain,
    expert_ids,
    route_scores,
    gate_weight,
    up_weight,
    down_weight,
    second_gain,
):
    q_heads, k_heads, v_heads = (
        lax.all_to_all(query_rows, "sp", split_axis=2, concat_axis=1, tiled=True),
        lax.all_to_all(key_rows, "sp", split_axis=2, concat_axis=1, tiled=True),
        lax.all_to_all(value_rows, "sp", split_axis=2, concat_axis=1, tiled=True),
    )
    attended = attend_local(q_heads[0], k_heads[0], v_heads[0], forget_sums[0])[None]
    returned_rows = lax.all_to_all(attended, "sp", split_axis=1, concat_axis=2, tiled=True)
    projected = jnp.dot(returned_rows[0], out_weight, preferred_element_type=jnp.float32)
    first_stream = layer_norm(
        deep_alpha * stream[0].astype(jnp.float32) + projected, first_gain
    ).astype(jnp.bfloat16)
    tokens_here = expert_ids.shape[1]
    top_k = expert_ids.shape[2]
    model_width = first_stream.shape[1]
    sp_count = lax.axis_size("sp")
    dp_count = lax.axis_size("dp")
    expert_count = sp_count * dp_count
    capacity = max(2, 3 * tokens_here * top_k // (2 * expert_count))
    flat_ids = expert_ids[0].reshape(-1)
    one_hot = (flat_ids[:, None] == jnp.arange(expert_count, dtype=jnp.int32)[None, :]).astype(
        jnp.int32
    )
    slot_ids = jnp.sum((jnp.cumsum(one_hot, axis=0) - one_hot) * one_hot, axis=1)
    slot_index = flat_ids * capacity + slot_ids
    slot_range = jnp.arange(expert_count * capacity, dtype=jnp.int32)
    matches = slot_range[:, None] == slot_index[None, :]
    dispatch = jnp.sum(matches.astype(jnp.int32).reshape(-1, tokens_here, top_k), axis=2).astype(
        jnp.bfloat16
    )
    outgoing = jnp.dot(dispatch, first_stream, preferred_element_type=jnp.float32).astype(
        jnp.bfloat16
    )
    outgoing = outgoing.reshape(expert_count, capacity, model_width)
    arrived = lax.all_to_all(outgoing, ("sp", "dp"), split_axis=0, concat_axis=0, tiled=True)
    finished = expert_rows(
        arrived.reshape(-1, model_width), gate_weight[0], up_weight[0], down_weight[0]
    )
    returned = lax.all_to_all(
        finished.reshape(arrived.shape), ("sp", "dp"), split_axis=0, concat_axis=0, tiled=True
    )
    route_weights = jax.nn.softmax(route_scores[0], axis=-1).reshape(-1)
    combine = jnp.sum(
        jnp.where(matches, route_weights[None, :], 0.0).reshape(-1, tokens_here, top_k), axis=2
    )
    mixture = lax.dot_general(
        combine,
        returned.reshape(-1, model_width).astype(jnp.float32),
        (((0,), (0,)), ((), ())),
        precision=lax.Precision.HIGHEST,
        preferred_element_type=jnp.float32,
    )
    second = layer_norm(deep_alpha * first_stream.astype(jnp.float32) + mixture, second_gain)
    return second.astype(jnp.bfloat16)[None]


def solution(mesh):
    return jax.shard_map(
        shards,
        mesh=mesh,
        in_specs=(
            P("dp", "sp", None),
            P("dp", "sp", None),
            P("dp", "sp", None),
            P("dp", "sp", None),
            P("dp", "sp", None),
            P(),
            P(),
            P("dp", "sp", None),
            P("dp", "sp", None),
            P(("sp", "dp"), None, None),
            P(("sp", "dp"), None, None),
            P(("sp", "dp"), None, None),
            P(),
        ),
        out_specs=P("dp", "sp", None),
        check_vma=False,
    )
```

profile of v0, /device:TPU:0, one launch (start us, length us, event | category | flops | bytes accessed | tf_op | source)
XLA Modules:
  0.0 323.6 jit_solution(11545134002252128617)
XLA Ops:
  0.0 2.5 copy.64
  2.5 0.5 broadcast.156
  3.0 12.3 %reduce.4 = bf16[2048,128]{1,0:T(8,128)(2,1)} reduce(bf16[2048,1,128]{2,1,0:T(2,128)(2,1)S(1)} %bitcast.124, bf16[]{:T(256)} %broadcast.156), dimensions={1}, to_apply=%bitcast.90.reduce_sub_computation | reduce | bytes 1048578
  15.3 2.0 reshape.161
  17.3 7.3 %all-to-all-start.1 = ((bf16[8,2,16384]{2,1,0:T(2,128)(2,1)}), bf16[8,2,16384]{2,1,0:T(2,128)(2,1)}, u32[]{:S(2)}, u32[]{:S(2)}) async-start(bf16[8,2,16384]{2,1,0:T(2,128)(2,1)} %reshape.161), calls=%async_computation.1 | async-start | bytes 1048576 | tf_op jit(solution)/shard_map/all_to_all | solution.py:86
  24.6 2.3 copy.66
  27.0 12.3 %reduce.5 = bf16[2048,128]{1,0:T(8,128)(2,1)} reduce(bf16[2048,1,128]{2,1,0:T(2,128)(2,1)S(1)} %bitcast.126, bf16[]{:T(256)} %broadcast.156), dimensions={1}, to_apply=%bitcast.92.reduce_sub_computation | reduce | bytes 1048578
  39.2 2.0 reshape.163
  41.2 17.2 %all-to-all-start.2 = ((bf16[8,2,16384]{2,1,0:T(2,128)(2,1)}), bf16[8,2,16384]{2,1,0:T(2,128)(2,1)}, u32[]{:S(2)}, u32[]{:S(2)}) async-start(bf16[8,2,16384]{2,1,0:T(2,128)(2,1)} %reshape.163), calls=%async_computation.2 | async-start | bytes 1048576 | tf_op jit(solution)/shard_map/all_to_all | solution.py:87
  58.5 2.4 copy.62
  60.8 12.3 %reduce.3 = bf16[2048,128]{1,0:T(8,128)(2,1)} reduce(bf16[2048,1,128]{2,1,0:T(2,128)(2,1)S(1)} %bitcast.127, bf16[]{:T(256)} %broadcast.156), dimensions={1}, to_apply=%bitcast.88.reduce_sub_computation | reduce | bytes 1048578
  73.1 2.0 reshape.159
  75.1 6.0 %all-to-all-start = ((bf16[8,2,16384]{2,1,0:T(2,128)(2,1)}), bf16[8,2,16384]{2,1,0:T(2,128)(2,1)}, u32[]{:S(2)}, u32[]{:S(2)}) async-start(bf16[8,2,16384]{2,1,0:T(2,128)(2,1)} %reshape.159), calls=%async_computation | async-start | bytes 1048576 | tf_op jit(solution)/shard_map/all_to_all | solution.py:85
  81.1 2.2 reshape.162
  83.4 0.3 copy.65
  83.7 0.2 reshape_squeeze.11
  84.0 1.0 copy.69
  85.0 2.2 reshape.164
  87.3 0.3 copy.67
  87.6 0.2 reshape_squeeze.12
  87.9 1.0 copy.70
  88.9 5.7 %all-to-all-done = bf16[8,2,16384]{2,1,0:T(2,128)(2,1)} async-done(((bf16[8,2,16384]{2,1,0:T(2,128)(2,1)}), bf16[8,2,16384]{2,1,0:T(2,128)(2,1)}, u32[]{:S(2)}, u32[]{:S(2)}) %all-to-all-start) | async-done | bytes 524320 | tf_op jit(solution)/shard_map/all_to_all | solution.py:85
  94.6 2.2 reshape.160
  96.9 0.3 copy.63
  97.2 1.0 reshape_squeeze.10
  98.3 18.2 %while.11 = (s32[]{:T(128)}, bf16[2,512,2,128]{3,2,1,0:T(2,128)(2,1)}, s32[2]{0:T(128)S(1)}, bf16[1024,2,128]{0,2,1:T(8,128)(2,1)}, bf16[1024,2,128]{2,0,1:T(8,1...) while((s32[]{:T(128)}, ...), condition=%wide.region_3.4_spmd.clone, body=%wide.region_0.3_spmd.clone.sunk | while | flops 555481600 | bytes 23138580 | solution.py:53
  98.3 0.6 dynamic_slice.23
  99.5 0.4 iota_compare_fusion.5
  99.9 2.8 fusion.70
  102.7 1.7 fusion.71
  104.4 1.9 fusion.72
  106.3 0.3 copy_dynamic-update-slice_fusion.2
  106.6 0.8 copy-done.3
  107.4 0.6 dynamic_slice.23
  108.6 0.4 iota_compare_fusion.5
  109.0 2.8 fusion.70
  111.7 1.7 fusion.71
  113.4 1.9 fusion.72
  115.3 0.3 copy_dynamic-update-slice_fusion.2
  115.7 0.8 copy-done.3
  116.4 3.6 %broadcast_in_dim_reshape.5 = bf16[1,1024,256]{2,0,1:T(2,128)(2,1)S(1)} reshape(bf16[2,512,2,128]{3,2,1,0:T(2,128)(2,1)} %get-tuple-element.52) | data formatting | bytes 1048576 | tf_op jit(solution)/shard_map/broadcast_in_dim;reshape | solution.py:89
  120.0 4.6 %reduce.6 = bf16[1024,256]{1,0:T(8,128)(2,1)} reduce(bf16[1024,1,256]{2,1,0:T(2,128)(2,1)S(1)} %bitcast.125, bf16[]{:T(256)} %broadcast.156), dimensions={1}, to_apply=%bitcast.94.reduce_sub_computation | reduce | bytes 1048578
  124.6 2.0 reshape.165
  126.6 4.3 %all-to-all-start.3 = ((bf16[8,2,16384]{2,1,0:T(2,128)(2,1)}), bf16[8,2,16384]{2,1,0:T(2,128)(2,1)}, u32[]{:S(2)}, u32[]{:S(2)}) async-start(bf16[8,2,16384]{2,1,0:T(2,128)(2,1)} %reshape.165), calls=%async_computation.3 | async-start | bytes 1048576 | tf_op jit(solution)/shard_map/all_to_all | solution.py:90
  131.3 1.2 reduce-window.6
  132.4 0.2 slice_reduce_fusion
  133.0 0.2 convert_reduce_fusion
  133.2 10.9 %all-to-all-done.3 = bf16[8,2,16384]{2,1,0:T(2,128)(2,1)} async-done(((bf16[8,2,16384]{2,1,0:T(2,128)(2,1)}), bf16[8,2,16384]{2,1,0:T(2,128)(2,1)}, u32[]{:S(2)}, u32[]{:S(2)}) %all-to-all-start.3) | async-done | bytes 524320 | tf_op jit(solution)/shard_map/all_to_all | solution.py:90
  144.1 2.2 reshape.166
  146.3 0.9 copy.85
  147.2 2.0 copy.73
  149.3 4.9 %fusion.51 = (f32[128]{0:T(128)S(1)}, f32[128,2048]{1,0:T(8,128)S(1)}) fusion(bf16[128,2048]{0,1:T(8,128)(2,1)} %bitcast.128, bf16[2048,2048]{1,0:T(8,128)(2,1)} %param.20, bf16[1,128,2048]{2,1,0:T(8,128)(2,1)} %param.15), kind=kOutput, calls=%fused_computation.66 | convolution fusion | flops 1074790272 | bytes 10486272 | tf_op jit(solution)/shard_map/dot_general | solution.py:91
  154.2 0.3 multiply_reduce_fusion.1
  154.5 1.1 convolution_convert_fusion.1
  155.6 74.7 %all_to_all.70 = bf16[32,24,2048]{2,1,0:T(8,128)(2,1)S(1)} all-to-all(bf16[32,24,2048]{2,1,0:T(8,128)(2,1)S(1)} %bitcast.119), channel_id=1, replica_groups=mesh['sp'=8,'dp'=4] {'sp','dp'}, dimensions={0} | all-to-all | bytes 6291456 | tf_op jit(solution)/shard_map/all_to_all | solution.py:117
  230.2 1.7 copy-done.1
  231.9 2.9 fusion.28
  234.9 8.3 %convolution_convert_fusion = bf16[768,2048]{1,0:T(8,128)(2,1)} fusion(bf16[1,512,2048]{2,1,0:T(8,128)(2,1)S(1)} %copy-done, f32[768,512]{1,0:T(8,128)} %fusion.28, bf16[768,2048]{1,0:T(8,128)(2,1)} %bitcast.131, bf16[1,2048,512]{2,1,0:T(8,128)(2,1)} %param.25), kind=kOutput, calls=%fused_computation.21 | convolution fusion | flops 3226730496 | bytes 12058624 | tf_op jit(solution)/shard_map/dot_general | solution.py:66
  243.2 3.8 %all-to-all-start.5 = ((bf16[32,24,2048]{2,1,0:T(8,128)(2,1)}), bf16[32,24,2048]{2,1,0:T(8,128)(2,1)}, u32[]{:S(2)}, u32[]{:S(2)}) async-start(bf16[32,24,2048]{2,1,0:T(8,128)(2,1)} %bitcast.129), calls=%async_computation.5 | async-start | bytes 6291456 | tf_op jit(solution)/shard_map/all_to_all | solution.py:121
  247.1 0.2 select_reduce_fusion
  247.3 71.1 %all-to-all-done.5 = bf16[32,24,2048]{2,1,0:T(8,128)(2,1)} async-done(((bf16[32,24,2048]{2,1,0:T(8,128)(2,1)}), bf16[32,24,2048]{2,1,0:T(8,128)(2,1)}, u32[]{:S(2)}, u32[]{:S(2)}) %all-to-all-start.5) | async-done | bytes 3145760 | tf_op jit(solution)/shard_map/all_to_all | solution.py:121
  318.3 3.6 %fusion.52 = (f32[128]{0:T(128)S(1)}, f32[128,2048]{1,0:T(8,128)S(1)}) fusion(f32[768,128]{1,0:T(8,128)S(1)} %select_reduce_fusion, bf16[768,2048]{1,0:T(8,128)(2,1)} %bitcast.16, f32[2048]{0:T(1024)S(1)} %copy-done.6, f32[128]{0:T(128)} %copy-done.9, f32[128,2048]{1,0:T(8,128)S(1)} %get-tuple-element.122, f32[128]{0:T(128)S(1)} %broadcast_multiply_fusion.1), kind=kOutput, calls=%fused_computation.67 | convolution fusion | flops 2418016256 | bytes 5645824 | tf_op jit(solution)/shard_map/dot_general | solution.py:128
  322.0 0.3 multiply_reduce_fusion
  322.2 1.0 fusion.38
  (55 shorter events, 1.1 us)
Async XLA Ops:
  0.0 234.9 %copy-start = (bf16[1,512,2048]{2,1,0:T(8,128)(2,1)S(1)}, bf16[1,512,2048]{2,1,0:T(8,128)(2,1)}, u32[]{:S(2)}) copy-start(bf16[1,512,2048]{2,1,0:T(8,128)(2,1)} %param.26) | copy-start | bytes 6291460
  17.3 23.9 %all-to-all-start.1 = ((bf16[8,2,16384]{2,1,0:T(2,128)(2,1)}), bf16[8,2,16384]{2,1,0:T(2,128)(2,1)}, u32[]{:S(2)}, u32[]{:S(2)}) async-start(bf16[8,2,16384]{2,1,0:T(2,128)(2,1)} %reshape.161), calls=%async_computation.1 | async-start | bytes 1048576 | tf_op jit(solution)/shard_map/all_to_all | solution.py:86
  41.2 33.9 %all-to-all-start.2 = ((bf16[8,2,16384]{2,1,0:T(2,128)(2,1)}), bf16[8,2,16384]{2,1,0:T(2,128)(2,1)}, u32[]{:S(2)}, u32[]{:S(2)}) async-start(bf16[8,2,16384]{2,1,0:T(2,128)(2,1)} %reshape.163), calls=%async_computation.2 | async-start | bytes 1048576 | tf_op jit(solution)/shard_map/all_to_all | solution.py:87
  75.1 19.5 %all-to-all-start = ((bf16[8,2,16384]{2,1,0:T(2,128)(2,1)}), bf16[8,2,16384]{2,1,0:T(2,128)(2,1)}, u32[]{:S(2)}, u32[]{:S(2)}) async-start(bf16[8,2,16384]{2,1,0:T(2,128)(2,1)} %reshape.159), calls=%async_computation | async-start | bytes 1048576 | tf_op jit(solution)/shard_map/all_to_all | solution.py:85
  87.9 10.4 %copy-start.5 = (f32[1,2,1024]{2,1,0:T(2,128)S(1)}, f32[1,2,1024]{2,1,0:T(2,128)}, u32[]{:S(2)}) copy-start(f32[1,2,1024]{2,1,0:T(2,128)} %param.19) | copy-start | bytes 24580
  102.6 1.7 copy-start.4
  104.3 1.9 copy-start.2
  106.6 0.8 copy-start.3
  111.7 1.7 copy-start.4
  113.4 1.9 copy-start.2
  115.6 0.8 copy-start.3
  116.4 14.5 %copy-start.10 = (s32[1,128,4]{1,2,0:T(4,128)S(1)}, s32[1,128,4]{1,2,0:T(4,128)}, u32[]{:S(2)}) copy-start(s32[1,128,4]{1,2,0:T(4,128)} %param.22) | copy-start | bytes 6148
  126.6 17.5 %all-to-all-start.3 = ((bf16[8,2,16384]{2,1,0:T(2,128)(2,1)}), bf16[8,2,16384]{2,1,0:T(2,128)(2,1)}, u32[]{:S(2)}, u32[]{:S(2)}) async-start(bf16[8,2,16384]{2,1,0:T(2,128)(2,1)} %reshape.165), calls=%async_computation.3 | async-start | bytes 1048576 | tf_op jit(solution)/shard_map/all_to_all | solution.py:90
  149.2 5.2 %copy-start.6 = (f32[2048]{0:T(1024)S(1)}, f32[2048]{0:T(1024)}, u32[]{:S(2)}) copy-start(f32[2048]{0:T(1024)} %param.21) | copy-start | bytes 24580
  154.5 75.8 %copy-start.9 = (f32[128]{0:T(128)}, f32[128]{0:T(128)S(1)}, u32[]{:S(2)}) copy-start(f32[128]{0:T(128)S(1)} %add_rsqrt_fusion.1) | copy-start | bytes 1540
  155.6 76.4 %copy-start.11 = (bf16[1,2048,512]{2,1,0:T(8,128)(2,1)S(1)}, bf16[1,2048,512]{2,1,0:T(8,128)(2,1)}, u32[]{:S(2)}) copy-start(bf16[1,2048,512]{2,1,0:T(8,128)(2,1)} %param.24) | copy-start | bytes 6291460
  230.2 1.7 copy-start.1
  243.2 3.8 %copy-start.7 = (f32[1,128,4]{1,2,0:T(4,128)S(1)}, f32[1,128,4]{1,2,0:T(4,128)}, u32[]{:S(2)}) copy-start(f32[1,128,4]{1,2,0:T(4,128)} %param.23) | copy-start | bytes 6148
  243.2 75.1 %all-to-all-start.5 = ((bf16[32,24,2048]{2,1,0:T(8,128)(2,1)}), bf16[32,24,2048]{2,1,0:T(8,128)(2,1)}, u32[]{:S(2)}, u32[]{:S(2)}) async-start(bf16[32,24,2048]{2,1,0:T(8,128)(2,1)} %bitcast.129), calls=%async_computation.5 | async-start | bytes 6291456 | tf_op jit(solution)/shard_map/all_to_all | solution.py:121
  318.3 3.9 %copy-start.8 = (f32[2048]{0:T(1024)S(1)}, f32[2048]{0:T(1024)}, u32[]{:S(2)}) copy-start(f32[2048]{0:T(1024)} %param.27) | copy-start | bytes 24580
where the time goes:
time: 327 us; the launch traced here: 324 us
  waiting for transfers between devices  87.6 us (27%)
  blocking collectives  74.7 us (23%)
  other arithmetic  48.9 us (15%)
  local copies, waits for them, and re-layouts  41.6 us (13%)
  starting transfers between devices  38.6 us (12%)
  matrix products  30.2 us (9%)
    all_to_all x1, blocking collectives, shards(): lax.all_to_all(outgoing, ('sp', 'dp'), split_axis=0, concat_axis=0, tiled...  74.7 us
    all_to_all x1, waiting for transfers between devices, shards(): lax.all_to_all(finished.reshape(arrived.shape), ('sp', 'dp'), split_axis=...  71.1 us
    unnamed x4, other arithmetic  41.5 us
    unnamed x37, local copies, waits for them, and re-layouts  29.4 us
    all_to_all x1, starting transfers between devices, shards(): lax.all_to_all(value_rows, 'sp', split_axis=2, concat_axis=1, tiled=True)  17.2 us
    all_to_all x1, waiting for transfers between devices, shards(): lax.all_to_all(attended, 'sp', split_axis=1, concat_axis=2, tiled=True)  10.9 us
    dot_general x1, matrix products, expert_rows(): jnp.dot(hidden, down_matrix, preferred_element_type=jnp.float32)  8.34 us
    all_to_all x1, starting transfers between devices, shards(): lax.all_to_all(key_rows, 'sp', split_axis=2, concat_axis=1, tiled=True)  7.31 us
  transfers between devices with their start and end apart: 5, of which 3 were waited for; matrix products, arithmetic and copies ran while one was open for 13% of the time, Pallas kernels for 0%

commit v1 on v0

--- a/solution.py
+++ b/solution.py
@@ -1,6 +1,10 @@
+import functools
+
 import jax
 import jax.numpy as jnp
 from jax import lax
+from jax.experimental import pallas as pl
+from jax.experimental.pallas import tpu as pltpu
 from jax.sharding import PartitionSpec as P
 
 deep_alpha = 8.0**0.25
@@ -16,41 +20,121 @@
     return (summed - centre) * lax.rsqrt(spread + norm_eps) * gain_row
 
 
-def attend_local(query_all, key_all, value_all, gate_all):
-    length, width = query_all.shape
-    heads = gate_all.shape[0]
-    head_size = width // heads
-    query_split = query_all.reshape(length, heads, head_size)
-    key_split = key_all.reshape(length, heads, head_size)
-    value_split = value_all.reshape(length, heads, head_size)
-    q_block = min(512, length)
-    block_count = length // q_block
+def attend_kernel(
+    sp_count, heads, head_size, q_ref, k_ref, v_ref, gate_ref, out_ref,
+    q_all, k_all, v_all, blended_all, in_send, in_recv, out_send, out_recv,
+):
+    me = lax.axis_index("sp")
+    rows = q_ref.shape[0]
+    length = rows * sp_count
+    mesh_id = pl.DeviceIdType.MESH
+
+    def cols(owner, head):
+        return pl.ds(pl.multiple_of((owner * heads + head) * head_size, head_size), head_size)
+
+    def band(owner):
+        return pl.ds(pl.multiple_of(owner * rows, rows), rows)
+
+    barrier = pltpu.get_barrier_semaphore()
+    for step in range(1, sp_count):
+        peer = lax.rem(me + step, sp_count)
+        pl.semaphore_signal(barrier, inc=1, device_id={"sp": peer}, device_id_type=mesh_id)
+    pl.semaphore_wait(barrier, sp_count - 1)
+
+    arrivals = []
+    pairs = ((q_ref, q_all), (k_ref, k_all), (v_ref, v_all))
+    for head in range(heads):
+        copies = []
+        for step in range(1, sp_count):
+            peer = lax.rem(me + step, sp_count)
+            for which, (src, dst) in enumerate(pairs):
+                copy = pltpu.make_async_remote_copy(
+                    src_ref=src.at[:, cols(peer, head)],
+                    dst_ref=dst.at[head, band(me), :],
+                    send_sem=in_send.at[head, which, step - 1],
+                    recv_sem=in_recv.at[head, which, step - 1],
+                    device_id={"sp": peer},
+                    device_id_type=mesh_id,
+                )
+                copy.start()
+                copies.append(copy)
+        arrivals.append(copies)
+    for head in range(heads):
+        for src, dst in pairs:
+            dst[head, band(me), :] = src[:, cols(me, head)]
+
+    q_block = min(256, length)
     inv_root = head_size ** (-0.5)
-    key_pos = jnp.arange(length, dtype=jnp.int32)
-
-    def one_block(block_index):
-        first_row = block_index * q_block
-        row_block = lax.dynamic_slice_in_dim(query_split, first_row, q_block, 0)
-        row_gate = lax.dynamic_slice_in_dim(gate_all, first_row, q_block, 1)
-        scores = (
-            jnp.einsum("qhd,khd->hqk", row_block, key_split, preferred_element_type=jnp.float32)
-            * inv_root
-        )
-        scores = scores + row_gate[:, :, None] - gate_all[:, None, :]
-        query_pos = first_row + jnp.arange(q_block, dtype=jnp.int32)
-        scores = jnp.where((query_pos[:, None] >= key_pos[None, :])[None], scores, mask_fill)
-        row_max = jnp.max(scores, axis=2, keepdims=True)
-        weights = jnp.exp(scores - row_max)
-        row_total = jnp.sum(weights, axis=2)
-        blended = jnp.einsum(
-            "hqk,khd->qhd",
-            weights.astype(jnp.bfloat16),
-            value_split,
-            preferred_element_type=jnp.float32,
-        )
-        return (blended / row_total.T[:, :, None]).astype(jnp.bfloat16)
-
-    return lax.map(one_block, jnp.arange(block_count, dtype=jnp.int32)).reshape(length, width)
+    departures = []
+    for head in range(heads):
+        for copy in arrivals[head]:
+            copy.wait_recv()
+        for block in range(length // q_block):
+            upto = (block + 1) * q_block
+            scores = (
+                lax.dot_general(
+                    q_all[head, block * q_block : upto, :],
+                    k_all[head, :upto, :],
+                    (((1,), (1,)), ((), ())),
+                    preferred_element_type=jnp.float32,
+                )
+                * inv_root
+                - gate_ref[head : head + 1, :upto]
+            )
+            q_pos = block * q_block + lax.broadcasted_iota(jnp.int32, scores.shape, 0)
+            k_pos = lax.broadcasted_iota(jnp.int32, scores.shape, 1)
+            scores = jnp.where(q_pos >= k_pos, scores, mask_fill)
+            weights = jnp.exp(scores - jnp.max(scores, axis=1, keepdims=True))
+            total = jnp.sum(weights, axis=1, keepdims=True)
+            blended = jnp.dot(
+                weights.astype(jnp.bfloat16),
+                v_all[head, :upto, :],
+                preferred_element_type=jnp.float32,
+            )
+            blended_all[head, block * q_block : upto, :] = (blended / total).astype(jnp.bfloat16)
+        for step in range(1, sp_count):
+            peer = lax.rem(me + step, sp_count)
+            copy = pltpu.make_async_remote_copy(
+                src_ref=blended_all.at[head, band(peer), :],
+                dst_ref=out_ref.at[:, cols(me, head)],
+                send_sem=out_send.at[head, step - 1],
+                recv_sem=out_recv.at[head, step - 1],
+                device_id={"sp": peer},
+                device_id_type=mesh_id,
+            )
+            copy.start()
+            departures.append(copy)
+        out_ref[:, cols(me, head)] = blended_all[head, band(me), :]
+    for copies in arrivals:
+        for copy in copies:
+            copy.wait_send()
+    for copy in departures:
+        copy.wait()
+
+
+def attend(query, key, value, gates, sp_count):
+    rows, width = query.shape
+    heads, length = gates.shape
+    head_size = width // (sp_count * heads)
+    whole = pltpu.VMEM((heads, length, head_size), jnp.bfloat16)
+    sems = pltpu.SemaphoreType.DMA
+    return pl.pallas_call(
+        functools.partial(attend_kernel, sp_count, heads, head_size),
+        out_shape=jax.ShapeDtypeStruct((rows, width), jnp.bfloat16),
+        in_specs=[pl.BlockSpec(memory_space=pltpu.VMEM)] * 4,
+        out_specs=pl.BlockSpec(memory_space=pltpu.VMEM),
+        scratch_shapes=[
+            whole, whole, whole, whole,
+            sems((heads, 3, sp_count - 1)),
+            sems((heads, 3, sp_count - 1)),
+            sems((heads, sp_count - 1)),
+            sems((heads, sp_count - 1)),
+        ],
+        compiler_params=pltpu.CompilerParams(
+            collective_id=0, has_side_effects=True, vmem_limit_bytes=40 * 2**20
+        ),
+        name="attend",
+    )(query, key, value, gates)
 
 
 def expert_rows(row_block, gate_matrix, up_matrix, down_matrix):
@@ -81,14 +165,10 @@
     down_weight,
     second_gain,
 ):
-    q_heads, k_heads, v_heads = (
-        lax.all_to_all(query_rows, "sp", split_axis=2, concat_axis=1, tiled=True),
-        lax.all_to_all(key_rows, "sp", split_axis=2, concat_axis=1, tiled=True),
-        lax.all_to_all(value_rows, "sp", split_axis=2, concat_axis=1, tiled=True),
-    )
-    attended = attend_local(q_heads[0], k_heads[0], v_heads[0], forget_sums[0])[None]
-    returned_rows = lax.all_to_all(attended, "sp", split_axis=1, concat_axis=2, tiled=True)
-    projected = jnp.dot(returned_rows[0], out_weight, preferred_element_type=jnp.float32)
+    attended = attend(
+        query_rows[0], key_rows[0], value_rows[0], forget_sums[0], lax.axis_size("sp")
+    )
+    projected = jnp.dot(attended, out_weight, preferred_element_type=jnp.float32)
     first_stream = layer_norm(
         deep_alpha * stream[0].astype(jnp.float32) + projected, first_gain
     ).astype(jnp.bfloat16)

time: 327 us -> 237 us (0.72)
  Pallas kernels: 0 us -> 55.4 us
  other arithmetic: 48.9 us -> 3.34 us
  starting transfers between devices: 38.6 us -> 3.77 us
  local copies, waits for them, and re-layouts: 41.6 us -> 7.1 us
  waiting for transfers between devices: 87.6 us -> 71.1 us
  matrix products: 30.2 us -> 20.8 us
    pallas_call x0 -> x1, Pallas kernels: none -> 55.4 us  [attend(): pl.pallas_call(functools.partial(attend_kernel, sp_count, heads, head_siz...]
    unnamed x4 -> x0, other arithmetic: 41.5 us -> none
    all_to_all x4 -> x0, starting transfers between devices: 34.9 us -> none  [the longest x1 17.2 us: shards(): lax.all_to_all(value_rows, 'sp', split_axis=2, concat_axis=1, tiled=True)]
    unnamed x37 -> x25, local copies, waits for them, and re-layouts: 29.4 us -> 6.49 us
    all_to_all x4 -> x0, waiting for transfers between devices: 16.6 us -> none  [the longest x1 10.9 us: shards(): lax.all_to_all(attended, 'sp', split_axis=1, concat_axis=2, tiled=True)]
    dot_general x5 -> x1, matrix products: 14.2 us -> 4.77 us  [shards(): jnp.dot(attended, out_weight, preferred_element_type=jnp.float32)]
    another operation x5 -> x1, local copies, waits for them, and re-layouts: 5.07 us -> 0.01 us  [the longest x1 3.57 us: shards(): attend_local(q_heads[0], k_heads[0], v_heads[0], forget_sums[0])[None]]
    reduce_sum x2 -> x0, other arithmetic: 3.35 us -> none  [one_block(): row_total = jnp.sum(weights, axis=2)]
  transfers between devices with their start and end apart: 5 -> 1, of which waited for: 3 -> 1; matrix products, arithmetic and copies ran while one was open for 13% -> 0% of each run, Pallas kernels for 0% -> 0%
where the time goes in v1:
time: 237 us; the launch traced here: 236 us
  blocking collectives  74.6 us (31%)
  waiting for transfers between devices  71.1 us (30%)
  Pallas kernels  55.4 us (23%)
  matrix products  20.8 us (9%)
  local copies, waits for them, and re-layouts  7.1 us (3%)
  starting transfers between devices  3.77 us (2%)
  other arithmetic  3.34 us (1%)
    all_to_all x1, blocking collectives, shards(): lax.all_to_all(outgoing, ('sp', 'dp'), split_axis=0, concat_axis=0, tiled...  74.6 us
    all_to_all x1, waiting for transfers between devices, shards(): lax.all_to_all(finished.reshape(arrived.shape), ('sp', 'dp'), split_axis=...  71.1 us
    pallas_call x1, Pallas kernels, attend(): pl.pallas_call(functools.partial(attend_kernel, sp_count, heads, head_siz...  55.4 us
    dot_general x1, matrix products, expert_rows(): jnp.dot(hidden, down_matrix, preferred_element_type=jnp.float32)  8.34 us
    unnamed x25, local copies, waits for them, and re-layouts  6.49 us
    dot_general x1, matrix products, shards(): jnp.dot(attended, out_weight, preferred_element_type=jnp.float32)  4.77 us
  transfers between devices with their start and end apart: 1, of which 1 were waited for; matrix products, arithmetic and copies ran while one was open for 0% of the time, Pallas kernels for 0%

profile of v1, /device:TPU:0, one launch (start us, length us, event | category | flops | bytes accessed | tf_op | source)
XLA Modules:
  0.0 236.2 jit_solution(7364911893790205650)
XLA Ops:
  0.0 0.0 copy-start
  0.0 0.9 copy.21
  0.9 0.1 eq.45
  1.0 0.1 eq.41
  1.2 1.2 reduce-window.6
  2.3 0.2 slice_reduce_fusion
  2.6 0.1 fusion.17
  2.7 0.1 reduce_sum.77
  2.9 0.1 copy.25
  2.9 0.2 convert_reduce_fusion
  3.1 0.0 copy-start.1
  3.1 1.0 copy-done.1
  4.2 0.0 copy-start.2
  4.2 1.0 copy-done.2
  5.2 0.0 copy-start.3
  5.2 1.0 copy-done.3
  6.3 0.0 copy-start.4
  6.3 0.7 copy-done.4
  7.0 0.0 copy-start.6
  7.0 55.4 %attend.1 = bf16[128,2048]{1,0:T(8,128)(2,1)S(1)} custom-call(bf16[128,2048]{1,0:T(8,128)(2,1)S(1)} %bitcast.60, bf16[128,2048]{1,0:T(8,128)(2,1)S(1)} %bitcast.61, bf16[128,2048]{1,0:T(8,128)(2,1)S(1)} %bitcast.62, f32[2,1024]{1,0:T(2,128)S(1)} %bitcast.63), custom_call_target="tpu_custom_call" | custom-call | tf_op jit(solution)/shard_map/attend/pallas_call | solution.py:121
  62.4 0.0 copy-done.6
  62.4 0.0 copy-start.7
  62.4 4.8 %fusion.26 = (f32[128]{0:T(128)S(1)}, f32[128,2048]{1,0:T(8,128)S(1)}) fusion(bf16[128,2048]{1,0:T(8,128)(2,1)S(1)} %attend.1, bf16[2048,2048]{1,0:T(8,128)(2,1)} %param.18, bf16[1,128,2048]{2,1,0:T(8,128)(2,1)S(1)} %copy-done.6), kind=kOutput, calls=%fused_computation.45 | convolution fusion | flops 1074790272 | bytes 10486272 | tf_op jit(solution)/shard_map/dot_general | solution.py:171
  67.2 0.3 multiply_reduce_fusion.1
  67.5 0.0 copy-done.7
  67.5 0.0 copy-start.10
  67.5 1.1 convolution_convert_fusion.1
  68.6 0.0 copy-done.10
  68.6 0.0 copy-start.11
  68.6 74.6 %all_to_all.10 = bf16[32,24,2048]{2,1,0:T(8,128)(2,1)S(1)} all-to-all(bf16[32,24,2048]{2,1,0:T(8,128)(2,1)S(1)} %bitcast.64), channel_id=1, replica_groups=mesh['sp'=8,'dp'=4] {'sp','dp'}, dimensions={0} | all-to-all | bytes 6291456 | tf_op jit(solution)/shard_map/all_to_all | solution.py:197
  143.1 0.0 copy-start.5
  143.1 1.7 copy-done.5
  144.8 0.0 copy-done.11
  144.8 3.0 %fusion.3 = f32[768,512]{1,0:T(8,128)} fusion(bf16[768,2048]{1,0:T(8,128)(2,1)S(1)} %bitcast.66, bf16[1,2048,512]{2,1,0:T(8,128)(2,1)S(1)} %copy-done.11), kind=kOutput, calls=%fused_computation.7 | convolution fusion | flops 1610612736 | bytes 6815744 | tf_op jit(solution)/shard_map/dot_general | solution.py:142
  147.8 0.0 copy-done
  147.8 8.3 %convolution_convert_fusion = bf16[768,2048]{1,0:T(8,128)(2,1)} fusion(bf16[1,512,2048]{2,1,0:T(8,128)(2,1)S(1)} %copy-done, f32[768,512]{1,0:T(8,128)} %fusion.3, bf16[768,2048]{1,0:T(8,128)(2,1)} %bitcast.67, bf16[1,2048,512]{2,1,0:T(8,128)(2,1)} %param.23), kind=kOutput, calls=%fused_computation | convolution fusion | flops 3226730496 | bytes 12058624 | tf_op jit(solution)/shard_map/dot_general | solution.py:150
  156.1 0.0 copy-start.8
  156.1 3.8 %all-to-all-start.1 = ((bf16[32,24,2048]{2,1,0:T(8,128)(2,1)}), bf16[32,24,2048]{2,1,0:T(8,128)(2,1)}, u32[]{:S(2)}, u32[]{:S(2)}) async-start(bf16[32,24,2048]{2,1,0:T(8,128)(2,1)} %bitcast.65), calls=%async_computation.1 | async-start | bytes 6291456 | tf_op jit(solution)/shard_map/all_to_all | solution.py:201
  159.9 0.0 copy-done.8
  160.0 0.2 select_reduce_fusion
  160.2 71.1 %all-to-all-done.1 = bf16[32,24,2048]{2,1,0:T(8,128)(2,1)} async-done(((bf16[32,24,2048]{2,1,0:T(8,128)(2,1)}), bf16[32,24,2048]{2,1,0:T(8,128)(2,1)}, u32[]{:S(2)}, u32[]{:S(2)}) %all-to-all-start.1) | async-done | bytes 3145760 | tf_op jit(solution)/shard_map/all_to_all | solution.py:201
  231.2 0.0 copy-start.9
  231.2 3.6 %fusion.27 = (f32[128]{0:T(128)S(1)}, f32[128,2048]{1,0:T(8,128)S(1)}) fusion(f32[768,128]{1,0:T(8,128)S(1)} %select_reduce_fusion, bf16[768,2048]{1,0:T(8,128)(2,1)} %bitcast.14, f32[2048]{0:T(1024)S(1)} %copy-done.7, f32[128]{0:T(128)} %copy-done.10, f32[128,2048]{1,0:T(8,128)S(1)} %get-tuple-element.6, f32[128]{0:T(128)S(1)} %broadcast_multiply_fusion.1), kind=kOutput, calls=%fused_computation.46 | convolution fusion | flops 2418016256 | bytes 5645824 | tf_op jit(solution)/shard_map/dot_general | solution.py:208
  234.9 0.3 multiply_reduce_fusion
  235.2 0.0 copy-done.9
  235.2 1.0 fusion.13
  (11 shorter events, 0.1 us)
Async XLA Ops:
  0.0 147.8 %copy-start = (bf16[1,512,2048]{2,1,0:T(8,128)(2,1)S(1)}, bf16[1,512,2048]{2,1,0:T(8,128)(2,1)}, u32[]{:S(2)}) copy-start(bf16[1,512,2048]{2,1,0:T(8,128)(2,1)} %param.24) | copy-start | bytes 6291460
  3.1 1.0 copy-start.1
  4.2 1.0 copy-start.2
  5.2 1.0 copy-start.3
  6.3 0.7 copy-start.4
  7.0 55.5 %copy-start.6 = (bf16[1,128,2048]{2,1,0:T(8,128)(2,1)S(1)}, bf16[1,128,2048]{2,1,0:T(8,128)(2,1)}, u32[]{:S(2)}) copy-start(bf16[1,128,2048]{2,1,0:T(8,128)(2,1)} %param.13) | copy-start | bytes 1572868
  62.4 5.1 %copy-start.7 = (f32[2048]{0:T(1024)S(1)}, f32[2048]{0:T(1024)}, u32[]{:S(2)}) copy-start(f32[2048]{0:T(1024)} %param.19) | copy-start | bytes 24580
  67.5 1.1 copy-start.10
  68.6 76.3 %copy-start.11 = (bf16[1,2048,512]{2,1,0:T(8,128)(2,1)S(1)}, bf16[1,2048,512]{2,1,0:T(8,128)(2,1)}, u32[]{:S(2)}) copy-start(bf16[1,2048,512]{2,1,0:T(8,128)(2,1)} %param.22) | copy-start | bytes 6291460
  143.1 1.7 copy-start.5
  156.1 3.8 %copy-start.8 = (f32[1,128,4]{1,2,0:T(4,128)S(1)}, f32[1,128,4]{1,2,0:T(4,128)}, u32[]{:S(2)}) copy-start(f32[1,128,4]{1,2,0:T(4,128)} %param.21) | copy-start | bytes 6148
  156.1 75.1 %all-to-all-start.1 = ((bf16[32,24,2048]{2,1,0:T(8,128)(2,1)}), bf16[32,24,2048]{2,1,0:T(8,128)(2,1)}, u32[]{:S(2)}, u32[]{:S(2)}) async-start(bf16[32,24,2048]{2,1,0:T(8,128)(2,1)} %bitcast.65), calls=%async_computation.1 | async-start | bytes 6291456 | tf_op jit(solution)/shard_map/all_to_all | solution.py:201
  231.2 3.9 %copy-start.9 = (f32[2048]{0:T(1024)S(1)}, f32[2048]{0:T(1024)}, u32[]{:S(2)}) copy-start(f32[2048]{0:T(1024)} %param.25) | copy-start | bytes 24580
